TPU v7x, 32 devices: a whole 2x2x4 slice. The times are simulated.
32 devices in a mesh: sp: 8 (over z, y), tp: 4 (over x, core).
Axes of the slice: x: 2, y: 2, z: 4, core: 2. Of those that a mesh axis runs over, the one named last changes fastest.
Arguments:
- skip_stream_vector: bfloat16 [8192, 2048], P(('sp', 'tp')), may hold values from -6 to 6
- probe_preactivation: bfloat16 [8192, 1024], P('sp', 'tp'), may hold values from -6 to 6
- retention_preactivation: bfloat16 [8192, 1024], P('sp', 'tp'), may hold values from -4.5 to 4.5
- content_vector: bfloat16 [8192, 1024], P('sp', 'tp'), may hold values from -6 to 6
- emission_preactivation: bfloat16 [8192, 1024], P('sp', 'tp'), may hold values from -6 to 6
- retention_slack: float32 [1024], P('tp'), may hold values from 0 to 0.12
- surge_rate: float32 [8192, 1024], P('sp', 'tp'), may hold values from -1.2 to 0
- subspace_scaling_factor: float32 [1024], P('tp'), may hold values from 0.1 to 1.9
- emission_matrix: bfloat16 [1024, 2048], replicated, may hold values from -0.1875 to 0.1875
- mlp_scaling_factor: float32 [2048], replicated, may hold values from 0.1 to 1.9
- switch_matrix: bfloat16 [2048, 5632], P('sp', 'tp'), may hold values from -0.125 to 0.125
- expansion_matrix: bfloat16 [2048, 5632], P('sp', 'tp'), may hold values from -0.125 to 0.125
- contraction_matrix: bfloat16 [5632, 2048], P('tp', 'sp'), may hold values from -0.078125 to 0.078125
Outputs:
- stream_out: bfloat16 [8192, 2048], P(('sp', 'tp'))
All inputs are finite; a program needn't handle non-finite values.
Results may differ from a plain program's by a relative error of at most 0.017.
Values may be sent and summed in bfloat16 or wider, within the bound.
A program may use at most 128 MiB of HBM per device.

v0:
```python
import functools

import jax
import jax.numpy as jnp
from jax import lax
from jax.experimental import pallas as pl
from jax.experimental.pallas import tpu as pltpu
from jax.sharding import PartitionSpec as P

HEAD_DIM = 128
BLOCK = 64
STATE_ROWS = HEAD_DIM + 16
EPSILON = 1e-06
MESH = pl.DeviceIdType.MESH
F32, BF16 = jnp.float32, jnp.bfloat16
LAST = (((1,), (1,)), ((), ()))
FIRST = (((0,), (0,)), ((), ()))


def weight_plan(n, me):
    out = []
    if n != 8:
        for tensor in range(3):
            for d in range(1, n):
                to, source = lax.rem(me + d, n), lax.rem(me + n - d, n)
                out.append((0, tensor, ("D", d, tensor), True, me, to, True, source, None))
        return out
    ny, nz = 2, n // 2
    z, y = me // ny, lax.rem(me, ny)

    def at(place, flip):
        return jnp.clip(place, 0, nz - 1) * ny + (1 - y if flip else y)

    def crossed(place, tensor, way):
        first, last = (1, nz - 1) if way > 0 else (nz - 2, 0)
        return (place == first) | (place == last) if tensor == 0 else place == first

    def inside(place):
        return (place >= 0) & (place < nz)

    for tensor in range(3):
        late = 1 if tensor == 2 else 0
        out.append((0, tensor, ("Y", 0, tensor), True, me, at(z, 1), True, at(z, 1), None))
        for way in (1, -1):
            for k in range(1, nz):
                to, unit = z + way, z + way - way * k
                name, above = (way, k, tensor), (way, k - 1, tensor)
                stage = 0 if k == 1 else k - 1 + late
                out.append(
                    (stage, tensor, name, inside(to) & inside(unit), at(unit, 0), at(to, 0),
                     inside(z - way * k), at(z - way * k, 0), None if k == 1 else above)
                )
                held = inside(z - way * k)
                if k == 1:
                    held = held & jnp.logical_not(crossed(z, tensor, way))
                out.append(
                    (k + late, tensor, ("Y", way * k, tensor), held, at(z - way * k, 0), at(z, 1),
                     held, at(z - way * k, 1), name)
                )
            out.append(
                (2, tensor, ("X", way, tensor), inside(z + way) & crossed(z + way, tensor, way), at(z, 1),
                 at(z + way, 0), crossed(z, tensor, way), at(z - way, 1), ("Y", 0, tensor))
            )
    return out


def kernel(
    n,
    m,
    skip_ref,
    query_ref,
    forget_ref,
    value_ref,
    emission_ref,
    slack_ref,
    surge_ref,
    gain_ref,
    projection_ref,
    row_gain_ref,
    switch_ref,
    expansion_ref,
    contraction_ref,
    out_ref,
    switch_all,
    expansion_all,
    contraction_all,
    projection,
    stream,
    normed,
    hidden,
    mixed,
    outputs,
    decayed_query,
    state,
    offset,
    state_out,
    state_in,
    part,
    from_buddy,
    cross_out,
    cross_in,
    local_sem,
    weight_send,
    weight_recv,
    skip_send,
    skip_recv,
    mixed_send,
    mixed_recv,
    state_send,
    state_recv,
    buddy_send,
    buddy_recv,
    cross_send,
    cross_recv,
):
    sp, tp = lax.axis_index("sp"), lax.axis_index("tp")
    tokens, width = query_ref.shape
    rows, model = skip_ref.shape
    depth, units = switch_ref.shape
    heads = width // HEAD_DIM
    pairs = m // 2

    barrier = pltpu.get_barrier_semaphore()
    for d in range(1, n):
        pl.semaphore_signal(barrier, inc=1, device_id=(lax.rem(sp + d, n), tp), device_id_type=MESH)
    for d in range(1, m):
        pl.semaphore_signal(barrier, inc=1, device_id=(sp, lax.rem(tp + d, m)), device_id_type=MESH)
    pl.semaphore_wait(barrier, n - 1 + m - 1)

    def remote(src, dst, send, recv, device):
        return pltpu.make_async_remote_copy(
            src_ref=src, dst_ref=dst, send_sem=send, recv_sem=recv, device_id=device, device_id_type=MESH
        )

    own_units = (switch_ref, expansion_ref, contraction_ref)

    def unit(tensor, owner):
        if tensor == 2:
            return contraction_all.at[owner]
        held = (switch_all, expansion_all)[tensor]
        return held.at[pl.ds(pl.multiple_of(owner * depth, depth), depth)]

    messages = {}
    for index, (stage, tensor, name, sent, owner, target, arrives, arriving, after) in enumerate(
        weight_plan(n, sp)
    ):
        src = own_units[tensor] if stage == 0 else unit(tensor, owner)
        args = (weight_send.at[index], weight_recv.at[index], (target, tp))
        send = remote(src, unit(tensor, owner), *args)
        arrival = remote(unit(tensor, arriving), unit(tensor, arriving), *args)
        messages[name] = (stage, sent, send, arrives, arrival, after)
    arrived = set()

    def where(condition, action):
        if condition is True:
            action()
        else:
            pl.when(condition)(action)

    def await_unit(name):
        if name not in arrived:
            arrived.add(name)
            where(messages[name][3], messages[name][4].wait_recv)

    def run_stage(wanted):
        for name, (stage, sent, send, _, _, after) in messages.items():
            if stage == wanted:
                if after is not None:
                    await_unit(after)
                where(sent, send.start)

    run_stage(0)

    def rows_of(owner):
        return pl.ds(pl.multiple_of(owner * rows, rows), rows)

    skip_sends, skip_arrivals, mixed_sends, mixed_arrivals = [], [], [], []
    for d in range(1, m):
        source, target = lax.rem(tp + m - d, m), (sp, lax.rem(tp + d, m))
        sems = (skip_send.at[d - 1], skip_recv.at[d - 1], target)
        skip_sends.append(remote(skip_ref, stream.at[rows_of(tp)], *sems))
        skip_arrivals.append(remote(stream.at[rows_of(source)], stream.at[rows_of(source)], *sems))
        sems = (mixed_send.at[d - 1], mixed_recv.at[d - 1], target)
        mixed_sends.append(remote(mixed.at[tp], mixed.at[tp], *sems))
        mixed_arrivals.append(remote(mixed.at[source], mixed.at[source], *sems))
    for copy in skip_sends:
        copy.start()
    local = [
        pltpu.make_async_copy(skip_ref, stream.at[rows_of(tp)], local_sem.at[0]),
        pltpu.make_async_copy(projection_ref, projection, local_sem.at[1]),
    ] + [pltpu.make_async_copy(own_units[t], unit(t, sp), local_sem.at[2 + t]) for t in range(3)]
    for copy in local:
        copy.start()

    state[...] = jnp.zeros_like(state)
    offset[...] = jnp.zeros_like(offset)
    before = lax.broadcasted_iota(jnp.int32, (BLOCK, BLOCK), 0) >= lax.broadcasted_iota(
        jnp.int32, (BLOCK, BLOCK), 1
    )
    lower = before.astype(F32)

    @pl.loop(0, tokens // BLOCK)
    def _(block):
        here = pl.ds(pl.multiple_of(block * BLOCK, BLOCK), BLOCK)
        raw = query_ref[here, :].astype(F32)
        query = raw * jax.nn.sigmoid(raw)
        gate = slack_ref[...] * jax.nn.sigmoid(-forget_ref[here, :].astype(F32))
        log_forget = jnp.log1p(-gate) + surge_ref[here, :]
        total = jnp.dot(lower, log_forget, precision=lax.Precision.HIGHEST, preferred_element_type=F32)
        middle, last = total[BLOCK // 2 : BLOCK // 2 + 1, :], total[BLOCK - 1 :, :]
        left = (query * jnp.exp(total - middle)).astype(BF16)
        right = (gate * jnp.exp(middle - total)).astype(BF16)
        carried = (query * jnp.exp(total)).astype(BF16)
        kept = (gate * jnp.exp(last - total)).astype(BF16)
        decayed_query[here, :] = (query * jnp.exp(total + offset[...])).astype(BF16)
        closing = jnp.exp(last)
        for head in range(heads):
            lanes = slice(head * HEAD_DIM, (head + 1) * HEAD_DIM)
            value = value_ref[here, lanes]
            scores = lax.dot_general(left[:, lanes], right[:, lanes], LAST, preferred_element_type=F32)
            scores = jnp.where(before, scores, 0.0).astype(BF16)
            held = state[head]
            outputs[here, lanes] = jnp.dot(
                scores, value, preferred_element_type=F32
            ) + lax.dot_general(carried[:, lanes], held.astype(BF16), LAST, preferred_element_type=F32)
            state[head] = closing[:, lanes] * held + lax.dot_general(
                value, kept[:, lanes], FIRST, preferred_element_type=F32
            )
        offset[...] += last

    for head in range(heads):
        lanes = slice(head * HEAD_DIM, (head + 1) * HEAD_DIM)
        state_out[head, :HEAD_DIM, :] = state[head].astype(BF16)
        decay = jnp.exp(offset[:, lanes])
        state_out[head, HEAD_DIM:, :] = jnp.broadcast_to(decay, (16, HEAD_DIM)).astype(BF16)
    state_copies = []
    for d in range(1, n):
        copy = remote(
            state_out,
            state_in.at[d - 1],
            state_send.at[d - 1],
            state_recv.at[d - 1],
            (lax.rem(sp + d, n), tp),
        )
        state_copies.append(copy)
        pl.when(sp + d < n)(copy.start)

    run_stage(1)

    for d in range(1, n):
        pl.when(sp >= d)(state_copies[d - 1].wait_recv)
    state[...] = jnp.zeros_like(state)

    @pl.loop(0, sp)
    def _(earlier):
        slot = sp - earlier - 1
        for head in range(heads):
            item = state_in[slot, head].astype(F32)
            state[head] = item[HEAD_DIM : HEAD_DIM + 1, :] * state[head] + item[:HEAD_DIM, :]

    tile = min(256, tokens)

    @pl.loop(0, tokens // tile)
    def _(turn):
        here = pl.ds(pl.multiple_of(turn * tile, tile), tile)
        for head in range(heads):
            lanes = slice(head * HEAD_DIM, (head + 1) * HEAD_DIM)
            full = outputs[here, lanes] + lax.dot_general(
                decayed_query[here, lanes], state[head].astype(BF16), LAST, preferred_element_type=F32
            )
            squares = jnp.mean(full * full, axis=-1, keepdims=True)
            raw = emission_ref[here, lanes].astype(F32)
            scaled = full * lax.rsqrt(squares + EPSILON) * gain_ref[:, lanes]
            mixed[tp, here, lanes] = (scaled * (raw * jax.nn.sigmoid(raw))).astype(BF16)

    for copy in mixed_sends:
        copy.start()
    run_stage(2)
    for copy in local:
        copy.wait()
    for copy in skip_arrivals:
        copy.wait_recv()
    for copy in mixed_arrivals:
        copy.wait_recv()

    @pl.loop(0, tokens // tile)
    def _(turn):
        here = pl.ds(pl.multiple_of(turn * tile, tile), tile)
        total = stream[here, :].astype(F32)
        for source in range(m):
            total += jnp.dot(
                mixed[source, here, :],
                projection[source * width : (source + 1) * width, :],
                preferred_element_type=F32,
            )
        rounded = total.astype(BF16)
        stream[here, :] = rounded
        total = rounded.astype(F32)
        squares = jnp.mean(total * total, axis=-1, keepdims=True)
        normed[here, :] = (total * lax.rsqrt(squares + EPSILON) * row_gain_ref[...]).astype(BF16)

    run_stage(3)
    for name in messages:
        if name[2] < 2:
            await_unit(name)

    core, pair = lax.rem(tp, 2), tp // 2
    buddy = (sp, pair * 2 + 1 - core)

    def half(number, which):
        return part.at[number, pl.ds(pl.multiple_of(which * rows, rows), rows)]

    def gate_and_up(number, owner):
        inputs = pl.ds(pl.multiple_of(owner * 2 * rows, 2 * rows), 2 * rows)

        def columns(lanes):
            value = normed[inputs, :]
            gate = jnp.dot(value, switch_all[:, lanes], preferred_element_type=F32)
            up = jnp.dot(value, expansion_all[:, lanes], preferred_element_type=F32)
            hidden[number, :, lanes] = (gate * jax.nn.sigmoid(gate) * up).astype(BF16)

        @pl.loop(0, units // 256)
        def _(turn):
            columns(pl.ds(pl.multiple_of(turn * 256, 256), 256))

        if units % 256:
            columns(slice(units // 256 * 256, units))

    def down(number):
        @pl.loop(0, n)
        def _(turn):
            lanes = pl.ds(pl.multiple_of(turn * depth, depth), depth)
            part[number, :, lanes] = jnp.dot(
                hidden[number], contraction_all[turn], preferred_element_type=F32
            ).astype(BF16)

        copy = remote(
            half(number, 1 - core),
            from_buddy.at[number],
            buddy_send.at[number],
            buddy_recv.at[number],
            buddy,
        )
        copy.start()
        return copy

    for d in [*range(1, pairs), 0]:
        gate_and_up(d, lax.rem(pair + d, pairs))
    run_stage(4)
    for name in messages:
        await_unit(name)
    tail = []
    for d in range(1, pairs):
        owner = lax.rem(pair + d, pairs)
        copy = down(d)
        copy.wait_recv()
        cross_out[d - 1] = (half(d, core)[...].astype(F32) + from_buddy[d].astype(F32)).astype(BF16)
        cross = remote(
            cross_out.at[d - 1],
            cross_in.at[d - 1],
            cross_send.at[d - 1],
            cross_recv.at[d - 1],
            (sp, owner * 2 + core),
        )
        cross.start()
        tail += [copy, cross]
    copy = down(0)
    copy.wait_recv()
    total = half(0, core)[...].astype(F32) + from_buddy[0].astype(F32) + stream[rows_of(tp), :].astype(F32)
    for d in range(1, pairs):
        tail[2 * d - 1].wait_recv()
        total += cross_in[d - 1].astype(F32)
    out_ref[...] = total.astype(BF16)

    for copy in tail + [copy] + skip_sends + mixed_sends:
        copy.wait_send()
    for _, sent, send, _, _, _ in messages.values():
        where(sent, send.wait_send)
    for d in range(1, n):
        pl.when(sp + d < n)(state_copies[d - 1].wait_send)


def on_device(n, m, *arrays):
    (skip, query, forget, value, emission, slack, surge, gain, projection, row_gain, switch, expansion, contraction) = arrays
    tokens, width = query.shape
    rows, model = skip.shape
    depth, units = switch.shape
    heads, pairs = width // HEAD_DIM, m // 2
    count = 3 * (3 * n // 2 + 3) if n == 8 else 3 * (n - 1)
    vmem, anywhere = pl.BlockSpec(memory_space=pltpu.VMEM), pl.BlockSpec(memory_space=pl.ANY)
    dma = pltpu.SemaphoreType.DMA
    return pl.pallas_call(
        functools.partial(kernel, n, m),
        out_shape=jax.ShapeDtypeStruct((rows, model), BF16),
        in_specs=[anywhere] + [vmem] * 7 + [anywhere, vmem] + [anywhere] * 3,
        out_specs=vmem,
        scratch_shapes=[
            pltpu.VMEM((model, units), BF16),
            pltpu.VMEM((model, units), BF16),
            pltpu.VMEM((n, units, depth), BF16),
            pltpu.VMEM(projection.shape, BF16),
            pltpu.VMEM((tokens, model), BF16),
            pltpu.VMEM((tokens, model), BF16),
            pltpu.VMEM((pairs, 2 * rows, units), BF16),
            pltpu.VMEM((m, tokens, width), BF16),
            pltpu.VMEM((tokens, width), F32),
            pltpu.VMEM((tokens, width), BF16),
            pltpu.VMEM((heads, HEAD_DIM, HEAD_DIM), F32),
            pltpu.VMEM((1, width), F32),
            pltpu.VMEM((heads, STATE_ROWS, HEAD_DIM), BF16),
            pltpu.VMEM((n - 1, heads, STATE_ROWS, HEAD_DIM), BF16),
            pltpu.VMEM((pairs, 2 * rows, model), BF16),
            pltpu.VMEM((pairs, rows, model), BF16),
            pltpu.VMEM((pairs - 1, rows, model), BF16),
            pltpu.VMEM((pairs - 1, rows, model), BF16),
            dma((5,)),
            dma((count,)),
            dma((count,)),
            dma((m - 1,)),
            dma((m - 1,)),
            dma((m - 1,)),
            dma((m - 1,)),
            dma((n - 1,)),
            dma((n - 1,)),
            dma((pairs,)),
            dma((pairs,)),
            dma((pairs - 1,)),
            dma((pairs - 1,)),
        ],
        compiler_params=pltpu.CompilerParams(
            collective_id=0, has_side_effects=True, vmem_limit_bytes=63_000_000
        ),
    )(
        skip,
        query,
        forget,
        value,
        emission,
        slack.reshape(1, width),
        surge,
        gain.reshape(1, width),
        projection,
        row_gain.reshape(1, model),
        switch,
        expansion,
        contraction,
    )


def solution(mesh):
    in_specs = (
        P(("sp", "tp"), None),
        P("sp", "tp"),
        P("sp", "tp"),
        P("sp", "tp"),
        P("sp", "tp"),
        P("tp"),
        P("sp", "tp"),
        P("tp"),
        P(),
        P(),
        P("sp", "tp"),
        P("sp", "tp"),
        P("tp", "sp"),
    )
    return jax.shard_map(
        functools.partial(on_device, mesh.shape["sp"], mesh.shape["tp"]),
        mesh=mesh,
        in_specs=in_specs,
        out_specs=P(("sp", "tp"), None),
        check_vma=False,
    )
```

profile of v0, /device:TPU:27, one launch (start us, length us, event | category | flops | bytes accessed | tf_op | source)
XLA Modules:
  0.0 220.8 jit_solution(17008401886491258566)
XLA Ops:
  0.0 218.5 %shard_map.127 = bf16[256,2048]{1,0:T(8,128)(2,1)} custom-call(bf16[256,2048]{1,0:T(8,128)(2,1)} %skip_ref.1, bf16[1024,256]{1,0:T(8,128)(2,1)} %query_ref.1, bf16[1024,256]{1,0:T(8,128)(2,1)} %forget_ref.1, bf16[1024,256]{1,0:T(8,128)(2,1)} %value_ref.1, bf16[1024,256]{1,0:T(8,128)(2,1)} %emission_ref.1, f32[1,256]{1,0:T(1,128)} %bitcast.4, ...), custom_call_target="tpu_custom_call" | custom-call | tf_op jit(solution)/shard_map/pallas_call | solution.py:392
  218.5 2.3 %copy.15 = bf16[256,2048]{1,0:T(8,128)(2,1)} copy(bf16[256,2048]{1,0:T(8,128)(2,1)} %shard_map.127) | data formatting | bytes 2097152
where the time goes:
time: 221 us
  Pallas kernels  219 us (99%)
  local copies, waits for them, and re-layouts  2.3 us (1%)
    pallas_call x1, Pallas kernels, on_device(): pl.pallas_call(functools.partial(kernel, n, m), out_shape=jax.ShapeDtypeS...  219 us

commit v1 on v0

--- a/solution.py
+++ b/solution.py
@@ -447,6 +447,569 @@
     )
 
 
+def paired_kernel(
+    n,
+    m,
+    skip_ref,
+    query_ref,
+    forget_ref,
+    value_ref,
+    emission_ref,
+    slack_ref,
+    surge_ref,
+    gain_ref,
+    projection_ref,
+    row_gain_ref,
+    switch_ref,
+    expansion_ref,
+    contraction_ref,
+    out_ref,
+    switch_half,
+    expansion_half,
+    contraction_half,
+    projection,
+    stream,
+    normed,
+    hidden,
+    mixed,
+    outputs,
+    decayed_query,
+    state,
+    offset,
+    state_out,
+    state_in,
+    chain_out,
+    chain_in,
+    part,
+    from_buddy,
+    cross_out,
+    cross_in,
+    plane_out,
+    plane_in,
+    local_sem,
+    weight_send,
+    weight_recv,
+    skip_sem,
+    state_sem,
+    chain_sem,
+    mixed_send,
+    mixed_recv,
+    normed_send,
+    normed_recv,
+    buddy_send,
+    buddy_recv,
+    cross_send,
+    cross_recv,
+    plane_send,
+    plane_recv,
+):
+    sp, tp = lax.axis_index("sp"), lax.axis_index("tp")
+    tokens, width = query_ref.shape
+    rows, model = skip_ref.shape
+    depth, units = switch_ref.shape
+    heads = width // HEAD_DIM
+    few = units // 256 * 128
+    many = units - few
+    z, y = sp // 2, lax.rem(sp, 2)
+    x, core = tp // 2, lax.rem(tp, 2)
+    planes = {0: z, 1: z + 1 - 2 * lax.rem(z, 2), 2: lax.rem(z + 2, 4), 3: 3 - z}
+    outer = (z == 0) | (z == 3)
+    beside = (z * 2 + 1 - y, tp)
+    across = (sp, (1 - x) * 2 + core)
+    buddy = (sp, x * 2 + 1 - core)
+    paired = (planes[1] * 2 + y, tp)
+
+    barrier = pltpu.get_barrier_semaphore()
+    for d in range(1, n):
+        pl.semaphore_signal(barrier, inc=1, device_id=(lax.rem(sp + d, n), tp), device_id_type=MESH)
+    for d in range(1, m):
+        pl.semaphore_signal(barrier, inc=1, device_id=(sp, lax.rem(tp + d, m)), device_id_type=MESH)
+    pl.semaphore_wait(barrier, n - 1 + m - 1)
+
+    def remote(src, dst, send, recv, device):
+        return pltpu.make_async_remote_copy(
+            src_ref=src, dst_ref=dst, send_sem=send, recv_sem=recv, device_id=device, device_id_type=MESH
+        )
+
+    sends = []
+
+    def start(copy):
+        copy.start()
+        sends.append(copy)
+
+    def by_kind(action):
+        pl.when(outer)(lambda: action(False))
+        pl.when(jnp.logical_not(outer))(lambda: action(True))
+
+    def own(tensor, big):
+        span = pl.ds(few, many) if big else pl.ds(0, few)
+        if tensor == 2:
+            return contraction_ref.at[span]
+        return (switch_ref, expansion_ref)[tensor].at[:, span]
+
+    def held(tensor, owner, big):
+        span = pl.ds(0, many if big else few)
+        if tensor == 2:
+            return contraction_half.at[owner, span]
+        place = pl.ds(pl.multiple_of(owner * depth, depth), depth)
+        return (switch_half, expansion_half)[tensor].at[place, span]
+
+    def weight(tensor, kind, big):
+        sems = (weight_send.at[tensor * 7 + kind], weight_recv.at[tensor * 7 + kind])
+        if kind == 0:
+            return remote(own(tensor, big), held(tensor, sp, big), *sems, beside)
+        if kind <= 3:
+            wanted = big if kind == 3 else not big
+            return remote(own(tensor, wanted), held(tensor, sp, wanted), *sems, (planes[kind] * 2 + y, tp))
+        unit = held(tensor, planes[kind - 3] * 2 + y, big)
+        return remote(unit, unit, *sems, beside)
+
+    def weight_arrival(tensor, kind, big):
+        sems = (weight_send.at[tensor * 7 + kind], weight_recv.at[tensor * 7 + kind])
+        if kind == 0:
+            owner = z * 2 + 1 - y
+        elif kind <= 3:
+            owner = planes[kind] * 2 + y
+        else:
+            owner = planes[kind - 3] * 2 + 1 - y
+        unit = held(tensor, owner, big)
+        return remote(unit, unit, *sems, beside)
+
+    def local_weight(tensor, big):
+        return pltpu.make_async_copy(own(tensor, big), held(tensor, sp, big), local_sem.at[2 + tensor])
+
+    def send_weights(*pairs):
+        def action(big):
+            for tensor, kind in pairs:
+                weight(tensor, kind, big).start()
+
+        by_kind(action)
+
+    def await_weights(*pairs):
+        def action(big):
+            for tensor, kind in pairs:
+                weight_arrival(tensor, kind, big).wait_recv()
+
+        by_kind(action)
+
+    def relay(tensor, kind):
+        def action(big):
+            weight_arrival(tensor, kind, big).wait_recv()
+            weight(tensor, kind + 3, big).start()
+
+        by_kind(action)
+
+    send_weights((0, 0), (0, 1), (0, 3), (0, 2), (1, 0))
+    start(remote(skip_ref, stream.at[1], skip_sem.at[0], skip_sem.at[1], across))
+    local = [
+        pltpu.make_async_copy(skip_ref, stream.at[0], local_sem.at[0]),
+        pltpu.make_async_copy(projection_ref, projection, local_sem.at[1]),
+    ]
+    for copy in local:
+        copy.start()
+
+    def prepare(big):
+        for tensor in range(3):
+            local_weight(tensor, big).start()
+        if not big and many > few:
+            switch_half[:, few:] = jnp.zeros((model, many - few), BF16)
+            expansion_half[:, few:] = jnp.zeros((model, many - few), BF16)
+            for owner in range(n):
+                contraction_half[owner, few:, :] = jnp.zeros((many - few, depth), BF16)
+
+    by_kind(prepare)
+
+    state[...] = jnp.zeros_like(state)
+    offset[...] = jnp.zeros_like(offset)
+    before = lax.broadcasted_iota(jnp.int32, (BLOCK, BLOCK), 0) >= lax.broadcasted_iota(
+        jnp.int32, (BLOCK, BLOCK), 1
+    )
+    lower = before.astype(F32)
+
+    def recur(block):
+        here = pl.ds(pl.multiple_of(block * BLOCK, BLOCK), BLOCK)
+        raw = query_ref[here, :].astype(F32)
+        query = raw * jax.nn.sigmoid(raw)
+        gate = slack_ref[...] * jax.nn.sigmoid(-forget_ref[here, :].astype(F32))
+        log_forget = jnp.log1p(-gate) + surge_ref[here, :]
+        total = jnp.dot(lower, log_forget, precision=lax.Precision.HIGHEST, preferred_element_type=F32)
+        middle, last = total[BLOCK // 2 : BLOCK // 2 + 1, :], total[BLOCK - 1 :, :]
+        left = (query * jnp.exp(total - middle)).astype(BF16)
+        right = (gate * jnp.exp(middle - total)).astype(BF16)
+        carried = (query * jnp.exp(total)).astype(BF16)
+        kept = (gate * jnp.exp(last - total)).astype(BF16)
+        decayed_query[here, :] = (query * jnp.exp(total + offset[...])).astype(BF16)
+        closing = jnp.exp(last)
+        for head in range(heads):
+            lanes = slice(head * HEAD_DIM, (head + 1) * HEAD_DIM)
+            value = value_ref[here, lanes]
+            scores = lax.dot_general(left[:, lanes], right[:, lanes], LAST, preferred_element_type=F32)
+            scores = jnp.where(before, scores, 0.0).astype(BF16)
+            kept_state = state[head]
+            outputs[here, lanes] = jnp.dot(
+                scores, value, preferred_element_type=F32
+            ) + lax.dot_general(carried[:, lanes], kept_state.astype(BF16), LAST, preferred_element_type=F32)
+            state[head] = closing[:, lanes] * kept_state + lax.dot_general(
+                value, kept[:, lanes], FIRST, preferred_element_type=F32
+            )
+        offset[...] += last
+
+    blocks = tokens // BLOCK
+    pl.loop(0, blocks * 5 // 8)(recur)
+    relay(0, 1)
+    pl.loop(blocks * 5 // 8, blocks)(recur)
+
+    for head in range(heads):
+        lanes = slice(head * HEAD_DIM, (head + 1) * HEAD_DIM)
+        state_out[head, :HEAD_DIM, :] = state[head].astype(BF16)
+        decay = jnp.exp(offset[:, lanes])
+        state_out[head, HEAD_DIM:, :] = jnp.broadcast_to(decay, (16, HEAD_DIM)).astype(BF16)
+    exchange = remote(state_out, state_in, state_sem.at[0], state_sem.at[1], beside)
+    start(exchange)
+    chain = remote(chain_out, chain_in, chain_sem.at[0], chain_sem.at[1], ((z + 1) * 2 + y, tp))
+    chain_arrival = remote(chain_in, chain_in, chain_sem.at[0], chain_sem.at[1], beside)
+    exchange.wait_recv()
+
+    @pl.when(z > 0)
+    def _():
+        chain_arrival.wait_recv()
+
+    @pl.when(z == 0)
+    def _():
+        chain_in[...] = jnp.zeros_like(chain_in)
+
+    for head in range(heads):
+        lanes = slice(head * HEAD_DIM, (head + 1) * HEAD_DIM)
+        decay = jnp.exp(offset[:, lanes])
+        other = state_in[head, :HEAD_DIM, :].astype(F32)
+        other_decay = state_in[head, HEAD_DIM : HEAD_DIM + 1, :].astype(F32)
+        prefix, mine = chain_in[head].astype(F32), state[head]
+
+        @pl.when(y == 0)
+        def _():
+            chain_out[head] = (other_decay * (decay * prefix + mine) + other).astype(BF16)
+            state[head] = prefix
+
+        @pl.when(y == 1)
+        def _():
+            middle = other_decay * prefix + other
+            chain_out[head] = (decay * middle + mine).astype(BF16)
+            state[head] = middle
+
+    pl.when(z < 3)(chain.start)
+    send_weights((1, 1), (1, 3), (1, 2))
+    relay(0, 3)
+    relay(0, 2)
+
+    def mixed_copy(slot, source, block, kind, device):
+        place = mixed.at[source, block]
+        index = kind * 2 + slot
+        return remote(place, place, mixed_send.at[index], mixed_recv.at[index], device)
+
+    for j in range(2):
+        side = 1 - x if j else x
+        for r in range(2):
+            target = 1 - core if r else core
+            block = side * 2 + target
+            here = pl.ds(pl.multiple_of(block * rows, rows), rows)
+            for head in range(heads):
+                lanes = slice(head * HEAD_DIM, (head + 1) * HEAD_DIM)
+                full = outputs[here, lanes] + lax.dot_general(
+                    decayed_query[here, lanes], state[head].astype(BF16), LAST, preferred_element_type=F32
+                )
+                squares = jnp.mean(full * full, axis=-1, keepdims=True)
+                raw = emission_ref[here, lanes].astype(F32)
+                scaled = full * lax.rsqrt(squares + EPSILON) * gain_ref[:, lanes]
+                mixed[tp, block, :, lanes] = (scaled * (raw * jax.nn.sigmoid(raw))).astype(BF16)
+            start(mixed_copy(1 - j, tp, block, r, (sp, (1 - x) * 2 + target)))
+            if r:
+                start(mixed_copy(j, tp, block, 2, buddy))
+
+    relay(1, 1)
+    for copy in local:
+        copy.wait()
+    remote(stream.at[1], stream.at[1], skip_sem.at[0], skip_sem.at[1], across).wait_recv()
+
+    half = rows // 2
+
+    def place_of(plane, side, which):
+        return (which * 4 + plane * 2 + side) * rows
+
+    def normed_copy(index, plane, side, which, device, piece=None):
+        first, count = place_of(plane, side, which), rows
+        target = place_of(1, side, which) if index < 2 else first
+        if piece is not None:
+            first, target, count = first + piece * half, target + piece * half, half
+        return remote(
+            normed.at[pl.ds(pl.multiple_of(first, half), count)],
+            normed.at[pl.ds(pl.multiple_of(target, half), count)],
+            normed_send.at[index],
+            normed_recv.at[index],
+            device,
+        )
+
+    def normed_arrival(index, plane, side, which, piece=None):
+        first, count = place_of(plane, side, which), rows
+        if piece is not None:
+            first, count = first + piece * half, half
+        block = normed.at[pl.ds(pl.multiple_of(first, half), count)]
+        return remote(block, block, normed_send.at[index], normed_recv.at[index], beside)
+
+    for j in range(2):
+        side = 1 - x if j else x
+        block = side * 2 + core
+        mixed_copy(j, (1 - x) * 2 + core, block, 0, across).wait_recv()
+        mixed_copy(j, (1 - x) * 2 + 1 - core, block, 1, across).wait_recv()
+        mixed_copy(j, x * 2 + 1 - core, block, 2, across).wait_recv()
+        first = place_of(0, side, core)
+        for piece in range(2):
+            here = slice(piece * half, (piece + 1) * half)
+            total = stream[j, here, :].astype(F32)
+            for source in range(m):
+                total += jnp.dot(
+                    mixed[source, block, here, :],
+                    projection[source * width : (source + 1) * width, :],
+                    preferred_element_type=F32,
+                )
+            rounded = total.astype(BF16)
+            stream[j, here, :] = rounded
+            total = rounded.astype(F32)
+            squares = jnp.mean(total * total, axis=-1, keepdims=True)
+            normed[pl.ds(pl.multiple_of(first + piece * half, half), half), :] = (
+                total * lax.rsqrt(squares + EPSILON) * row_gain_ref[...]
+            ).astype(BF16)
+            if j == 0:
+                start(normed_copy(piece, 0, side, core, paired, piece))
+        start(normed_copy(2 + j, 0, side, core, buddy))
+
+    send_weights((2, 1), (2, 3), (2, 2))
+    relay(1, 3)
+    relay(1, 2)
+    send_weights((2, 0))
+
+    def tiles(plane, action):
+        @pl.loop(0, 2)
+        def _(which):
+            here = pl.ds(pl.multiple_of(which * 4 * rows + plane * 2 * rows, 2 * rows), 2 * rows)
+
+            @pl.loop(0, many // 256)
+            def _(turn):
+                action(here, pl.ds(pl.multiple_of(turn * 256, 256), 256))
+
+            if many % 256:
+                action(here, slice(many // 256 * 256, many))
+
+    def gate(here, lanes):
+        value = jnp.dot(normed[here, :], switch_half[:, lanes], preferred_element_type=F32)
+        hidden[here, lanes] = (value * jax.nn.sigmoid(value)).astype(BF16)
+
+    def up(here, lanes):
+        value = jnp.dot(normed[here, :], expansion_half[:, lanes], preferred_element_type=F32)
+        hidden[here, lanes] = (hidden[here, lanes].astype(F32) * value).astype(BF16)
+
+    for j in range(2):
+        normed_arrival(2 + j, 0, 1 - x if j else x, 1 - core).wait_recv()
+
+    def await_local(big):
+        for tensor in range(3):
+            local_weight(tensor, big).wait()
+
+    by_kind(await_local)
+    await_weights((0, 0), (0, 4), (0, 6), (0, 5))
+    tiles(0, gate)
+    for piece in range(2):
+        normed_arrival(piece, 1, x, core, piece).wait_recv()
+        start(normed_copy(4 + piece, 1, x, core, across, piece))
+        start(normed_copy(6 + piece, 1, x, core, buddy, piece))
+    await_weights((1, 0), (1, 4), (1, 6), (1, 5))
+    tiles(0, up)
+    for piece in range(2):
+        normed_arrival(4 + piece, 1, 1 - x, core, piece).wait_recv()
+        start(normed_copy(8 + piece, 1, 1 - x, core, buddy, piece))
+    relay(2, 1)
+    for piece in range(2):
+        normed_arrival(6 + piece, 1, x, 1 - core, piece).wait_recv()
+    for piece in range(2):
+        normed_arrival(8 + piece, 1, 1 - x, 1 - core, piece).wait_recv()
+    tiles(1, gate)
+    tiles(1, up)
+
+    base = z // 2
+
+    def owner_of(turn):
+        group, even = turn // 2, lax.rem(turn, 2)
+        pair = base + (group // 2) * (1 - 2 * base)
+        return (pair * 2 + even) * 2 + y + lax.rem(group, 2) * (1 - 2 * y)
+
+    mine = pl.multiple_of(core * 4 * rows, 4 * rows)
+    theirs = pl.multiple_of((1 - core) * 4 * rows, 4 * rows)
+
+    def buddy_copy(turn):
+        return remote(
+            part.at[turn, pl.ds(theirs, 4 * rows)],
+            from_buddy.at[turn],
+            buddy_send.at[turn],
+            buddy_recv.at[turn],
+            buddy,
+        )
+
+    def cross_copy(turn):
+        return remote(cross_out.at[turn], cross_in.at[turn], cross_send.at[turn], cross_recv.at[turn], across)
+
+    def plane_copy(turn):
+        return remote(plane_out.at[turn], plane_in.at[turn], plane_send.at[turn], plane_recv.at[turn], paired)
+
+    def share(turn, plane, side):
+        place = (plane * 2 + side) * rows
+        local_part = part[turn, pl.ds(pl.multiple_of(mine + place, rows), rows), :].astype(F32)
+        return local_part + from_buddy[turn, pl.ds(pl.multiple_of(place, rows), rows), :].astype(F32)
+
+    lag_cross, lag_plane = 3, 5
+
+    @pl.loop(0, n + lag_plane)
+    def _(step):
+        @pl.when(step == 1)
+        def _():
+            relay(2, 3)
+
+        @pl.when(step == 2)
+        def _():
+            await_weights((2, 0), (2, 4))
+            relay(2, 2)
+
+        @pl.when(step == 6)
+        def _():
+            await_weights((2, 5), (2, 6))
+
+        @pl.when(step < n)
+        def _():
+            unit = contraction_half.at[owner_of(step)]
+
+            @pl.loop(0, 4)
+            def _(turn):
+                here = pl.ds(pl.multiple_of(turn * 2 * rows, 2 * rows), 2 * rows)
+                part[step, here, :] = jnp.dot(
+                    hidden[here, :], unit[...], preferred_element_type=F32
+                ).astype(BF16)
+
+            buddy_copy(step).start()
+
+        @pl.when((step >= 1) & (step < n + 1))
+        def _():
+            turn = step - 1
+            buddy_copy(turn).wait_recv()
+            for plane in range(2):
+                cross_out[turn, plane] = share(turn, plane, 1 - x).astype(BF16)
+            cross_copy(turn).start()
+
+        @pl.when((step >= lag_cross) & (step < n + lag_cross))
+        def _():
+            turn = step - lag_cross
+            cross_copy(turn).wait_recv()
+            plane_out[turn] = (share(turn, 1, x) + cross_in[turn, 1].astype(F32)).astype(BF16)
+            plane_copy(turn).start()
+
+        @pl.when(step >= lag_plane)
+        def _():
+            turn = step - lag_plane
+            plane_copy(turn).wait_recv()
+            lanes = pl.ds(pl.multiple_of(owner_of(turn) * depth, depth), depth)
+            total = stream[0, :, lanes].astype(F32) + share(turn, 0, x)
+            total += cross_in[turn, 0].astype(F32) + plane_in[turn].astype(F32)
+            out_ref[:, lanes] = total.astype(BF16)
+
+    @pl.loop(0, n)
+    def _(turn):
+        buddy_copy(turn).wait_send()
+        cross_copy(turn).wait_send()
+        plane_copy(turn).wait_send()
+
+    for copy in sends:
+        copy.wait_send()
+
+    def await_weight_sends(big):
+        for tensor in range(3):
+            for kind in range(7):
+                weight(tensor, kind, big).wait_send()
+
+    by_kind(await_weight_sends)
+    pl.when(z < 3)(chain.wait_send)
+
+
+def on_device_paired(n, m, *arrays):
+    (skip, query, forget, value, emission, slack, surge, gain, projection, row_gain, switch, expansion, contraction) = arrays
+    tokens, width = query.shape
+    rows, model = skip.shape
+    depth, units = switch.shape
+    heads = width // HEAD_DIM
+    many = units - units // 256 * 128
+    vmem, anywhere = pl.BlockSpec(memory_space=pltpu.VMEM), pl.BlockSpec(memory_space=pl.ANY)
+    dma = pltpu.SemaphoreType.DMA
+    return pl.pallas_call(
+        functools.partial(paired_kernel, n, m),
+        out_shape=jax.ShapeDtypeStruct((rows, model), BF16),
+        in_specs=[anywhere] + [vmem] * 7 + [anywhere, vmem] + [anywhere] * 3,
+        out_specs=vmem,
+        scratch_shapes=[
+            pltpu.VMEM((model, many), BF16),
+            pltpu.VMEM((model, many), BF16),
+            pltpu.VMEM((n, many, depth), BF16),
+            pltpu.VMEM(projection.shape, BF16),
+            pltpu.VMEM((2, rows, model), BF16),
+            pltpu.VMEM((2 * tokens, model), BF16),
+            pltpu.VMEM((2 * tokens, many), BF16),
+            pltpu.VMEM((m, m, rows, width), BF16),
+            pltpu.VMEM((tokens, width), F32),
+            pltpu.VMEM((tokens, width), BF16),
+            pltpu.VMEM((heads, HEAD_DIM, HEAD_DIM), F32),
+            pltpu.VMEM((1, width), F32),
+            pltpu.VMEM((heads, STATE_ROWS, HEAD_DIM), BF16),
+            pltpu.VMEM((heads, STATE_ROWS, HEAD_DIM), BF16),
+            pltpu.VMEM((heads, HEAD_DIM, HEAD_DIM), BF16),
+            pltpu.VMEM((heads, HEAD_DIM, HEAD_DIM), BF16),
+            pltpu.VMEM((n, 2 * tokens, depth), BF16),
+            pltpu.VMEM((n, tokens, depth), BF16),
+            pltpu.VMEM((n, 2, rows, depth), BF16),
+            pltpu.VMEM((n, 2, rows, depth), BF16),
+            pltpu.VMEM((n, rows, depth), BF16),
+            pltpu.VMEM((n, rows, depth), BF16),
+            dma((5,)),
+            dma((21,)),
+            dma((21,)),
+            dma((2,)),
+            dma((2,)),
+            dma((2,)),
+            dma((6,)),
+            dma((6,)),
+            dma((10,)),
+            dma((10,)),
+            dma((n,)),
+            dma((n,)),
+            dma((n,)),
+            dma((n,)),
+            dma((n,)),
+            dma((n,)),
+        ],
+        compiler_params=pltpu.CompilerParams(
+            collective_id=0, has_side_effects=True, vmem_limit_bytes=64_000_000
+        ),
+    )(
+        skip,
+        query,
+        forget,
+        value,
+        emission,
+        slack.reshape(1, width),
+        surge,
+        gain.reshape(1, width),
+        projection,
+        row_gain.reshape(1, model),
+        switch,
+        expansion,
+        contraction,
+    )
+
+
 def solution(mesh):
     in_specs = (
         P(("sp", "tp"), None),
@@ -463,8 +1026,9 @@
         P("sp", "tp"),
         P("tp", "sp"),
     )
+    n, m = mesh.shape["sp"], mesh.shape["tp"]
     return jax.shard_map(
-        functools.partial(on_device, mesh.shape["sp"], mesh.shape["tp"]),
+        functools.partial(on_device_paired if (n, m) == (8, 4) else on_device, n, m),
         mesh=mesh,
         in_specs=in_specs,
         out_specs=P(("sp", "tp"), None),

time: 221 us -> 180 us (0.81)
  the two profiles are of different devices: /device:TPU:27 before, /device:TPU:16 now
where the time goes in v1:
time: 180 us
  Pallas kernels  177 us (98%)
  local copies, waits for them, and re-layouts  2.3 us (1%)
    pallas_call x1, Pallas kernels, on_device_paired(): pl.pallas_call(functools.partial(paired_kernel, n, m), out_shape=jax.Shap...  177 us

profile of v1, /device:TPU:16, one launch (start us, length us, event | category | flops | bytes accessed | tf_op | source)
XLA Modules:
  0.0 179.7 jit_solution(10929351751057226885)
XLA Ops:
  0.0 177.4 %shard_map.127 = bf16[256,2048]{1,0:T(8,128)(2,1)} custom-call(bf16[256,2048]{1,0:T(8,128)(2,1)} %skip_ref.1, bf16[1024,256]{1,0:T(8,128)(2,1)} %query_ref.1, bf16[1024,256]{1,0:T(8,128)(2,1)} %forget_ref.1, bf16[1024,256]{1,0:T(8,128)(2,1)} %value_ref.1, bf16[1024,256]{1,0:T(8,128)(2,1)} %emission_ref.1, f32[1,256]{1,0:T(1,128)} %bitcast.4, ...), custom_call_target="tpu_custom_call" | custom-call | tf_op jit(solution)/shard_map/pallas_call | solution.py:948
  177.4 2.3 %copy.15 = bf16[256,2048]{1,0:T(8,128)(2,1)} copy(bf16[256,2048]{1,0:T(8,128)(2,1)} %shard_map.127) | data formatting | bytes 2097152

commit v2 on v1

--- a/solution.py
+++ b/solution.py
@@ -524,8 +524,6 @@
         pl.semaphore_signal(barrier, inc=1, device_id=(lax.rem(sp + d, n), tp), device_id_type=MESH)
     for d in range(1, m):
         pl.semaphore_signal(barrier, inc=1, device_id=(sp, lax.rem(tp + d, m)), device_id_type=MESH)
-    pl.semaphore_wait(barrier, n - 1 + m - 1)
-
     def remote(src, dst, send, recv, device):
         return pltpu.make_async_remote_copy(
             src_ref=src, dst_ref=dst, send_sem=send, recv_sem=recv, device_id=device, device_id_type=MESH
@@ -555,17 +553,19 @@
         return (switch_half, expansion_half)[tensor].at[place, span]
 
     def weight(tensor, kind, big):
-        sems = (weight_send.at[tensor * 7 + kind], weight_recv.at[tensor * 7 + kind])
+        sems = (weight_send.at[tensor * 8 + kind], weight_recv.at[tensor * 8 + kind])
         if kind == 0:
             return remote(own(tensor, big), held(tensor, sp, big), *sems, beside)
         if kind <= 3:
             wanted = big if kind == 3 else not big
             return remote(own(tensor, wanted), held(tensor, sp, wanted), *sems, (planes[kind] * 2 + y, tp))
-        unit = held(tensor, planes[kind - 3] * 2 + y, big)
+        unit = held(tensor, planes[1 if kind == 7 else kind - 3] * 2 + y, big)
+        if kind == 7:
+            return remote(unit, unit, sems[0], weight_recv.at[tensor * 8 + 2], (planes[3] * 2 + y, tp))
         return remote(unit, unit, *sems, beside)
 
     def weight_arrival(tensor, kind, big):
-        sems = (weight_send.at[tensor * 7 + kind], weight_recv.at[tensor * 7 + kind])
+        sems = (weight_send.at[tensor * 8 + kind], weight_recv.at[tensor * 8 + kind])
         if kind == 0:
             owner = z * 2 + 1 - y
         elif kind <= 3:
@@ -581,7 +581,8 @@
     def send_weights(*pairs):
         def action(big):
             for tensor, kind in pairs:
-                weight(tensor, kind, big).start()
+                if big or kind != 2:
+                    weight(tensor, kind, big).start()
 
         by_kind(action)
 
@@ -599,8 +600,6 @@
 
         by_kind(action)
 
-    send_weights((0, 0), (0, 1), (0, 3), (0, 2), (1, 0))
-    start(remote(skip_ref, stream.at[1], skip_sem.at[0], skip_sem.at[1], across))
     local = [
         pltpu.make_async_copy(skip_ref, stream.at[0], local_sem.at[0]),
         pltpu.make_async_copy(projection_ref, projection, local_sem.at[1]),
@@ -655,9 +654,22 @@
         offset[...] += last
 
     blocks = tokens // BLOCK
-    pl.loop(0, blocks * 5 // 8)(recur)
-    relay(0, 1)
-    pl.loop(blocks * 5 // 8, blocks)(recur)
+    early = blocks // 4
+    pl.loop(0, early)(recur)
+    pl.semaphore_wait(barrier, n - 1 + m - 1)
+    send_weights((0, 0), (0, 1))
+    pl.when(z > 0)(lambda: send_weights((0, 3)))
+
+    @pl.when(z > 1)
+    def _():
+        send_weights((0, 2))
+
+    @pl.when(z == 3)
+    def _():
+        send_weights((1, 1), (1, 3))
+
+    start(remote(skip_ref, stream.at[1], skip_sem.at[0], skip_sem.at[1], across))
+    pl.loop(early, blocks)(recur)
 
     for head in range(heads):
         lanes = slice(head * HEAD_DIM, (head + 1) * HEAD_DIM)
@@ -668,38 +680,61 @@
     start(exchange)
     chain = remote(chain_out, chain_in, chain_sem.at[0], chain_sem.at[1], ((z + 1) * 2 + y, tp))
     chain_arrival = remote(chain_in, chain_in, chain_sem.at[0], chain_sem.at[1], beside)
+    relay(0, 1)
     exchange.wait_recv()
+
+    def forward(tensor):
+        pl.when(jnp.logical_not(outer))(lambda: weight(tensor, 7, True).start())
+
+    pl.when(z == 2)(lambda: forward(0))
+
+    def advance(prefixes):
+        for head in range(heads):
+            lanes = slice(head * HEAD_DIM, (head + 1) * HEAD_DIM)
+            decay = jnp.exp(offset[:, lanes])
+            other = state_in[head, :HEAD_DIM, :].astype(F32)
+            other_decay = state_in[head, HEAD_DIM : HEAD_DIM + 1, :].astype(F32)
+            prefix, mine = prefixes(head), state[head]
+
+            @pl.when(y == 0)
+            def _():
+                chain_out[head] = (other_decay * (decay * prefix + mine) + other).astype(BF16)
+                state[head] = prefix
+
+            @pl.when(y == 1)
+            def _():
+                middle = other_decay * prefix + other
+                chain_out[head] = (decay * middle + mine).astype(BF16)
+                state[head] = middle
+
+    @pl.when(z == 0)
+    def _():
+        advance(lambda head: jnp.zeros((HEAD_DIM, HEAD_DIM), F32))
+        chain.start()
+        send_weights((0, 3), (1, 1), (1, 3))
+
+    @pl.when((z == 1) | (z == 2))
+    def _():
+        pl.when(z == 1)(lambda: send_weights((1, 1)))
+        pl.when(z == 2)(lambda: send_weights((1, 3), (1, 2)))
+
+    relay(0, 3)
 
     @pl.when(z > 0)
     def _():
         chain_arrival.wait_recv()
-
-    @pl.when(z == 0)
+        advance(lambda head: chain_in[head].astype(F32))
+
+    pl.when((z > 0) & (z < 3))(chain.start)
+
+    @pl.when(z == 1)
     def _():
-        chain_in[...] = jnp.zeros_like(chain_in)
-
-    for head in range(heads):
-        lanes = slice(head * HEAD_DIM, (head + 1) * HEAD_DIM)
-        decay = jnp.exp(offset[:, lanes])
-        other = state_in[head, :HEAD_DIM, :].astype(F32)
-        other_decay = state_in[head, HEAD_DIM : HEAD_DIM + 1, :].astype(F32)
-        prefix, mine = chain_in[head].astype(F32), state[head]
-
-        @pl.when(y == 0)
-        def _():
-            chain_out[head] = (other_decay * (decay * prefix + mine) + other).astype(BF16)
-            state[head] = prefix
-
-        @pl.when(y == 1)
-        def _():
-            middle = other_decay * prefix + other
-            chain_out[head] = (decay * middle + mine).astype(BF16)
-            state[head] = middle
-
-    pl.when(z < 3)(chain.start)
-    send_weights((1, 1), (1, 3), (1, 2))
-    relay(0, 3)
-    relay(0, 2)
+        send_weights((0, 2))
+        forward(0)
+        send_weights((1, 3), (1, 2))
+
+    pl.when(z == 2)(lambda: send_weights((1, 1)))
+    send_weights((1, 0))
 
     def mixed_copy(slot, source, block, kind, device):
         place = mixed.at[source, block]
@@ -725,35 +760,30 @@
             if r:
                 start(mixed_copy(j, tp, block, 2, buddy))
 
-    relay(1, 1)
     for copy in local:
         copy.wait()
     remote(stream.at[1], stream.at[1], skip_sem.at[0], skip_sem.at[1], across).wait_recv()
 
-    half = rows // 2
+    pieces = 4
+    fine = rows // pieces
 
     def place_of(plane, side, which):
         return (which * 4 + plane * 2 + side) * rows
 
-    def normed_copy(index, plane, side, which, device, piece=None):
+    def normed_rows(plane, side, which, piece):
         first, count = place_of(plane, side, which), rows
-        target = place_of(1, side, which) if index < 2 else first
         if piece is not None:
-            first, target, count = first + piece * half, target + piece * half, half
+            first, count = first + piece * fine, fine
+        return normed.at[pl.ds(pl.multiple_of(first, fine), count)]
+
+    def normed_copy(index, device, plane, side, which, piece=None, target=None):
         return remote(
-            normed.at[pl.ds(pl.multiple_of(first, half), count)],
-            normed.at[pl.ds(pl.multiple_of(target, half), count)],
+            normed_rows(plane, side, which, piece),
+            normed_rows(plane if target is None else target, side, which, piece),
             normed_send.at[index],
             normed_recv.at[index],
             device,
         )
-
-    def normed_arrival(index, plane, side, which, piece=None):
-        first, count = place_of(plane, side, which), rows
-        if piece is not None:
-            first, count = first + piece * half, half
-        block = normed.at[pl.ds(pl.multiple_of(first, half), count)]
-        return remote(block, block, normed_send.at[index], normed_recv.at[index], beside)
 
     for j in range(2):
         side = 1 - x if j else x
@@ -763,7 +793,7 @@
         mixed_copy(j, x * 2 + 1 - core, block, 2, across).wait_recv()
         first = place_of(0, side, core)
         for piece in range(2):
-            here = slice(piece * half, (piece + 1) * half)
+            here = slice(piece * rows // 2, (piece + 1) * rows // 2)
             total = stream[j, here, :].astype(F32)
             for source in range(m):
                 total += jnp.dot(
@@ -775,17 +805,18 @@
             stream[j, here, :] = rounded
             total = rounded.astype(F32)
             squares = jnp.mean(total * total, axis=-1, keepdims=True)
-            normed[pl.ds(pl.multiple_of(first + piece * half, half), half), :] = (
+            normed[pl.ds(pl.multiple_of(first + piece * rows // 2, rows // 2), rows // 2), :] = (
                 total * lax.rsqrt(squares + EPSILON) * row_gain_ref[...]
             ).astype(BF16)
             if j == 0:
-                start(normed_copy(piece, 0, side, core, paired, piece))
-        start(normed_copy(2 + j, 0, side, core, buddy))
-
-    send_weights((2, 1), (2, 3), (2, 2))
+                for part_of in range(piece * pieces // 2, (piece + 1) * pieces // 2):
+                    start(normed_copy(2 + part_of, paired, 0, side, core, part_of, 1))
+        start(normed_copy(j, buddy, 0, side, core))
+
+    relay(0, 2)
+    relay(1, 1)
+    forward(1)
     relay(1, 3)
-    relay(1, 2)
-    send_weights((2, 0))
 
     def tiles(plane, action):
         @pl.loop(0, 2)
@@ -807,8 +838,11 @@
         value = jnp.dot(normed[here, :], expansion_half[:, lanes], preferred_element_type=F32)
         hidden[here, lanes] = (hidden[here, lanes].astype(F32) * value).astype(BF16)
 
+    def normed_arrives(index, plane, side, which, piece=None):
+        normed_copy(index, buddy, plane, side, which, piece).wait_recv()
+
     for j in range(2):
-        normed_arrival(2 + j, 0, 1 - x if j else x, 1 - core).wait_recv()
+        normed_arrives(j, 0, 1 - x if j else x, 1 - core)
 
     def await_local(big):
         for tensor in range(3):
@@ -817,20 +851,22 @@
     by_kind(await_local)
     await_weights((0, 0), (0, 4), (0, 6), (0, 5))
     tiles(0, gate)
-    for piece in range(2):
-        normed_arrival(piece, 1, x, core, piece).wait_recv()
-        start(normed_copy(4 + piece, 1, x, core, across, piece))
-        start(normed_copy(6 + piece, 1, x, core, buddy, piece))
+    relay(1, 2)
+    for piece in range(pieces):
+        normed_arrives(2 + piece, 1, x, core, piece)
+        start(normed_copy(6 + piece, across, 1, x, core, piece))
+        start(normed_copy(10 + piece, buddy, 1, x, core, piece))
+    send_weights((2, 0), (2, 1), (2, 3), (2, 2))
     await_weights((1, 0), (1, 4), (1, 6), (1, 5))
     tiles(0, up)
-    for piece in range(2):
-        normed_arrival(4 + piece, 1, 1 - x, core, piece).wait_recv()
-        start(normed_copy(8 + piece, 1, 1 - x, core, buddy, piece))
+    for piece in range(pieces):
+        normed_arrives(6 + piece, 1, 1 - x, core, piece)
+        start(normed_copy(14 + piece, buddy, 1, 1 - x, core, piece))
     relay(2, 1)
-    for piece in range(2):
-        normed_arrival(6 + piece, 1, x, 1 - core, piece).wait_recv()
-    for piece in range(2):
-        normed_arrival(8 + piece, 1, 1 - x, 1 - core, piece).wait_recv()
+    forward(2)
+    for piece in range(pieces):
+        normed_arrives(10 + piece, 1, x, 1 - core, piece)
+        normed_arrives(14 + piece, 1, 1 - x, 1 - core, piece)
     tiles(1, gate)
     tiles(1, up)
 
@@ -853,11 +889,16 @@
             buddy,
         )
 
+    def partner(odd):
+        return (sp + (paired[0] - sp) * odd, across[1] + (tp - across[1]) * odd)
+
     def cross_copy(turn):
-        return remote(cross_out.at[turn], cross_in.at[turn], cross_send.at[turn], cross_recv.at[turn], across)
+        sems = (cross_send.at[turn], cross_recv.at[turn])
+        return remote(cross_out.at[turn], cross_in.at[turn], *sems, partner(lax.rem(turn, 2)))
 
     def plane_copy(turn):
-        return remote(plane_out.at[turn], plane_in.at[turn], plane_send.at[turn], plane_recv.at[turn], paired)
+        sems = (plane_send.at[turn], plane_recv.at[turn])
+        return remote(plane_out.at[turn], plane_in.at[turn], *sems, partner(1 - lax.rem(turn, 2)))
 
     def share(turn, plane, side):
         place = (plane * 2 + side) * rows
@@ -898,15 +939,18 @@
         def _():
             turn = step - 1
             buddy_copy(turn).wait_recv()
-            for plane in range(2):
-                cross_out[turn, plane] = share(turn, plane, 1 - x).astype(BF16)
+            odd = lax.rem(turn, 2)
+            cross_out[turn, 0] = share(turn, odd, 1 - x + (2 * x - 1) * odd).astype(BF16)
+            cross_out[turn, 1] = share(turn, 1, 1 - x).astype(BF16)
             cross_copy(turn).start()
 
         @pl.when((step >= lag_cross) & (step < n + lag_cross))
         def _():
             turn = step - lag_cross
             cross_copy(turn).wait_recv()
-            plane_out[turn] = (share(turn, 1, x) + cross_in[turn, 1].astype(F32)).astype(BF16)
+            odd = lax.rem(turn, 2)
+            total = share(turn, 1 - odd, x + (1 - 2 * x) * odd) + cross_in[turn, 1].astype(F32)
+            plane_out[turn] = total.astype(BF16)
             plane_copy(turn).start()
 
         @pl.when(step >= lag_plane)
@@ -929,7 +973,7 @@
 
     def await_weight_sends(big):
         for tensor in range(3):
-            for kind in range(7):
+            for kind in range(8) if big else (0, 1, 3, 4, 5, 6):
                 weight(tensor, kind, big).wait_send()
 
     by_kind(await_weight_sends)
@@ -974,15 +1018,15 @@
             pltpu.VMEM((n, rows, depth), BF16),
             pltpu.VMEM((n, rows, depth), BF16),
             dma((5,)),
-            dma((21,)),
-            dma((21,)),
+            dma((24,)),
+            dma((24,)),
             dma((2,)),
             dma((2,)),
             dma((2,)),
             dma((6,)),
             dma((6,)),
-            dma((10,)),
-            dma((10,)),
+            dma((18,)),
+            dma((18,)),
             dma((n,)),
             dma((n,)),
             dma((n,)),

time: 180 us -> 157 us (0.87)
  Pallas kernels: 177 us -> 154 us
    pallas_call x1, Pallas kernels: 177 us -> 154 us  [on_device_paired(): pl.pallas_call(functools.partial(paired_kernel, n, m), out_shape=jax.Shap...]
where the time goes in v2:
time: 157 us
  Pallas kernels  154 us (98%)
  local copies, waits for them, and re-layouts  2.3 us (1%)
    pallas_call x1, Pallas kernels, on_device_paired(): pl.pallas_call(functools.partial(paired_kernel, n, m), out_shape=jax.Shap...  154 us

profile of v2, /device:TPU:16, one launch (start us, length us, event | category | flops | bytes accessed | tf_op | source)
XLA Modules:
  0.0 156.6 jit_solution(18187283323970713477)
XLA Ops:
  0.0 154.3 %shard_map.127 = bf16[256,2048]{1,0:T(8,128)(2,1)} custom-call(bf16[256,2048]{1,0:T(8,128)(2,1)} %skip_ref.1, bf16[1024,256]{1,0:T(8,128)(2,1)} %query_ref.1, bf16[1024,256]{1,0:T(8,128)(2,1)} %forget_ref.1, bf16[1024,256]{1,0:T(8,128)(2,1)} %value_ref.1, bf16[1024,256]{1,0:T(8,128)(2,1)} %emission_ref.1, f32[1,256]{1,0:T(1,128)} %bitcast.4, ...), custom_call_target="tpu_custom_call" | custom-call | tf_op jit(solution)/shard_map/pallas_call | solution.py:992
  154.3 2.3 %copy.15 = bf16[256,2048]{1,0:T(8,128)(2,1)} copy(bf16[256,2048]{1,0:T(8,128)(2,1)} %shard_map.127) | data formatting | bytes 2097152

commit v3 on v2

--- a/solution.py
+++ b/solution.py
@@ -491,7 +491,8 @@
     weight_recv,
     skip_sem,
     state_sem,
-    chain_sem,
+    chain_send,
+    chain_recv,
     mixed_send,
     mixed_recv,
     normed_send,
@@ -657,7 +658,9 @@
     early = blocks // 4
     pl.loop(0, early)(recur)
     pl.semaphore_wait(barrier, n - 1 + m - 1)
-    send_weights((0, 0), (0, 1))
+    send_weights((0, 0))
+    pl.when(z == 0)(lambda: send_weights((0, 3)))
+    send_weights((0, 1))
     pl.when(z > 0)(lambda: send_weights((0, 3)))
 
     @pl.when(z > 1)
@@ -678,63 +681,50 @@
         state_out[head, HEAD_DIM:, :] = jnp.broadcast_to(decay, (16, HEAD_DIM)).astype(BF16)
     exchange = remote(state_out, state_in, state_sem.at[0], state_sem.at[1], beside)
     start(exchange)
-    chain = remote(chain_out, chain_in, chain_sem.at[0], chain_sem.at[1], ((z + 1) * 2 + y, tp))
-    chain_arrival = remote(chain_in, chain_in, chain_sem.at[0], chain_sem.at[1], beside)
-    relay(0, 1)
+    def chain(distance):
+        sems = (chain_send.at[distance - 1], chain_recv.at[distance - 1])
+        return remote(chain_out, chain_in.at[distance - 1], *sems, ((z + distance) * 2 + y, tp))
+
     exchange.wait_recv()
+    for head in range(heads):
+        lanes = slice(head * HEAD_DIM, (head + 1) * HEAD_DIM)
+        decay = jnp.exp(offset[:, lanes])
+        other = state_in[head, :HEAD_DIM, :].astype(F32)
+        other_decay = state_in[head, HEAD_DIM : HEAD_DIM + 1, :].astype(F32)
+        later = jnp.where(y == 0, other, state[head])
+        earlier = jnp.where(y == 0, state[head], other)
+        later_decay = jnp.where(y == 0, other_decay, decay)
+        chain_out[head, :HEAD_DIM, :] = (later_decay * earlier + later).astype(BF16)
+        chain_out[head, HEAD_DIM:, :] = jnp.broadcast_to(decay * other_decay, (16, HEAD_DIM)).astype(BF16)
+    for distance in range(1, 4):
+        pl.when(z + distance < 4)(chain(distance).start)
 
     def forward(tensor):
         pl.when(jnp.logical_not(outer))(lambda: weight(tensor, 7, True).start())
 
-    pl.when(z == 2)(lambda: forward(0))
-
-    def advance(prefixes):
-        for head in range(heads):
-            lanes = slice(head * HEAD_DIM, (head + 1) * HEAD_DIM)
-            decay = jnp.exp(offset[:, lanes])
-            other = state_in[head, :HEAD_DIM, :].astype(F32)
-            other_decay = state_in[head, HEAD_DIM : HEAD_DIM + 1, :].astype(F32)
-            prefix, mine = prefixes(head), state[head]
-
-            @pl.when(y == 0)
-            def _():
-                chain_out[head] = (other_decay * (decay * prefix + mine) + other).astype(BF16)
-                state[head] = prefix
-
-            @pl.when(y == 1)
-            def _():
-                middle = other_decay * prefix + other
-                chain_out[head] = (decay * middle + mine).astype(BF16)
-                state[head] = middle
-
-    @pl.when(z == 0)
-    def _():
-        advance(lambda head: jnp.zeros((HEAD_DIM, HEAD_DIM), F32))
-        chain.start()
-        send_weights((0, 3), (1, 1), (1, 3))
+    pl.when(z == 0)(lambda: send_weights((1, 1), (1, 3)))
 
     @pl.when((z == 1) | (z == 2))
     def _():
-        pl.when(z == 1)(lambda: send_weights((1, 1)))
-        pl.when(z == 2)(lambda: send_weights((1, 3), (1, 2)))
-
-    relay(0, 3)
-
-    @pl.when(z > 0)
-    def _():
-        chain_arrival.wait_recv()
-        advance(lambda head: chain_in[head].astype(F32))
-
-    pl.when((z > 0) & (z < 3))(chain.start)
-
-    @pl.when(z == 1)
-    def _():
-        send_weights((0, 2))
-        forward(0)
-        send_weights((1, 3), (1, 2))
-
-    pl.when(z == 2)(lambda: send_weights((1, 1)))
+        pl.when(z == 1)(lambda: send_weights((0, 2)))
+        send_weights((1, 1))
+
     send_weights((1, 0))
+    for distance in range(1, 4):
+        pl.when(z >= distance)(chain(distance).wait_recv)
+    for head in range(heads):
+        state[head] = jnp.zeros((HEAD_DIM, HEAD_DIM), F32)
+        for distance in range(3, 0, -1):
+
+            @pl.when(z >= distance)
+            def _():
+                item = chain_in[distance - 1, head].astype(F32)
+                state[head] = item[HEAD_DIM : HEAD_DIM + 1, :] * state[head] + item[:HEAD_DIM, :]
+
+        @pl.when(y == 1)
+        def _():
+            item = state_in[head].astype(F32)
+            state[head] = item[HEAD_DIM : HEAD_DIM + 1, :] * state[head] + item[:HEAD_DIM, :]
 
     def mixed_copy(slot, source, block, kind, device):
         place = mixed.at[source, block]
@@ -759,6 +749,17 @@
             start(mixed_copy(1 - j, tp, block, r, (sp, (1 - x) * 2 + target)))
             if r:
                 start(mixed_copy(j, tp, block, 2, buddy))
+
+    relay(0, 1)
+    forward(0)
+    pl.when(jnp.logical_not(outer))(lambda: send_weights((1, 3)))
+    relay(0, 3)
+
+    @pl.when(jnp.logical_not(outer))
+    def _():
+        relay(1, 1)
+        forward(1)
+        send_weights((1, 2))
 
     for copy in local:
         copy.wait()
@@ -813,15 +814,17 @@
                     start(normed_copy(2 + part_of, paired, 0, side, core, part_of, 1))
         start(normed_copy(j, buddy, 0, side, core))
 
+    pl.when(outer)(lambda: relay(1, 1))
+    pl.when(jnp.logical_not(outer))(lambda: send_weights((2, 3)))
     relay(0, 2)
-    relay(1, 1)
-    forward(1)
-    relay(1, 3)
-
-    def tiles(plane, action):
+
+    def tiles(plane, action, side=None):
+        count = rows if side is not None else 2 * rows
+        first = plane * 2 * rows + (0 if side is None else side * rows)
+
         @pl.loop(0, 2)
         def _(which):
-            here = pl.ds(pl.multiple_of(which * 4 * rows + plane * 2 * rows, 2 * rows), 2 * rows)
+            here = pl.ds(pl.multiple_of(which * 4 * rows + first, rows), count)
 
             @pl.loop(0, many // 256)
             def _(turn):
@@ -841,34 +844,50 @@
     def normed_arrives(index, plane, side, which, piece=None):
         normed_copy(index, buddy, plane, side, which, piece).wait_recv()
 
-    for j in range(2):
-        normed_arrives(j, 0, 1 - x if j else x, 1 - core)
+    def pass_on(piece):
+        normed_arrives(2 + piece, 1, x, core, piece)
+        start(normed_copy(6 + piece, across, 1, x, core, piece))
+        start(normed_copy(10 + piece, buddy, 1, x, core, piece))
 
     def await_local(big):
         for tensor in range(3):
             local_weight(tensor, big).wait()
 
     by_kind(await_local)
+    pass_on(0)
+    relay(1, 3)
+    pass_on(1)
+    for j in range(2):
+        normed_arrives(j, 0, 1 - x if j else x, 1 - core)
     await_weights((0, 0), (0, 4), (0, 6), (0, 5))
     tiles(0, gate)
-    relay(1, 2)
+    pass_on(2)
+    pl.when(z < 3)(lambda: relay(1, 2))
+    pass_on(3)
+    pl.when(z == 3)(lambda: relay(1, 2))
+    send_weights((2, 1), (2, 0))
+    pl.when(outer)(lambda: send_weights((2, 3)))
+    send_weights((2, 2))
     for piece in range(pieces):
-        normed_arrives(2 + piece, 1, x, core, piece)
-        start(normed_copy(6 + piece, across, 1, x, core, piece))
-        start(normed_copy(10 + piece, buddy, 1, x, core, piece))
-    send_weights((2, 0), (2, 1), (2, 3), (2, 2))
+        normed_arrives(10 + piece, 1, x, 1 - core, piece)
+    tiles(1, gate, x)
     await_weights((1, 0), (1, 4), (1, 6), (1, 5))
     tiles(0, up)
     for piece in range(pieces):
         normed_arrives(6 + piece, 1, 1 - x, core, piece)
         start(normed_copy(14 + piece, buddy, 1, 1 - x, core, piece))
-    relay(2, 1)
-    forward(2)
+    tiles(1, up, x)
+
+    @pl.when(z < 3)
+    def _():
+        relay(2, 1)
+        forward(2)
+
     for piece in range(pieces):
-        normed_arrives(10 + piece, 1, x, 1 - core, piece)
         normed_arrives(14 + piece, 1, 1 - x, 1 - core, piece)
-    tiles(1, gate)
-    tiles(1, up)
+    tiles(1, gate, 1 - x)
+    tiles(1, up, 1 - x)
+    pl.when(z == 3)(lambda: relay(2, 1))
 
     base = z // 2
 
@@ -909,13 +928,13 @@
 
     @pl.loop(0, n + lag_plane)
     def _(step):
-        @pl.when(step == 1)
-        def _():
-            relay(2, 3)
-
         @pl.when(step == 2)
         def _():
             await_weights((2, 0), (2, 4))
+            relay(2, 3)
+
+        @pl.when(step == 4)
+        def _():
             relay(2, 2)
 
         @pl.when(step == 6)
@@ -977,7 +996,8 @@
                 weight(tensor, kind, big).wait_send()
 
     by_kind(await_weight_sends)
-    pl.when(z < 3)(chain.wait_send)
+    for distance in range(1, 4):
+        pl.when(z + distance < 4)(chain(distance).wait_send)
 
 
 def on_device_paired(n, m, *arrays):
@@ -1009,8 +1029,8 @@
             pltpu.VMEM((1, width), F32),
             pltpu.VMEM((heads, STATE_ROWS, HEAD_DIM), BF16),
             pltpu.VMEM((heads, STATE_ROWS, HEAD_DIM), BF16),
-            pltpu.VMEM((heads, HEAD_DIM, HEAD_DIM), BF16),
-            pltpu.VMEM((heads, HEAD_DIM, HEAD_DIM), BF16),
+            pltpu.VMEM((heads, STATE_ROWS, HEAD_DIM), BF16),
+            pltpu.VMEM((3, heads, STATE_ROWS, HEAD_DIM), BF16),
             pltpu.VMEM((n, 2 * tokens, depth), BF16),
             pltpu.VMEM((n, tokens, depth), BF16),
             pltpu.VMEM((n, 2, rows, depth), BF16),
@@ -1022,7 +1042,8 @@
             dma((24,)),
             dma((2,)),
             dma((2,)),
-            dma((2,)),
+            dma((3,)),
+            dma((3,)),
             dma((6,)),
             dma((6,)),
             dma((18,)),

time: 157 us -> 152 us (0.968)
  Pallas kernels: 154 us -> 150 us
    pallas_call x1, Pallas kernels: 154 us -> 150 us  [on_device_paired(): pl.pallas_call(functools.partial(paired_kernel, n, m), out_shape=jax.Shap...]
where the time goes in v3:
time: 152 us
  Pallas kernels  150 us (99%)
  local copies, waits for them, and re-layouts  2.3 us (2%)
    pallas_call x1, Pallas kernels, on_device_paired(): pl.pallas_call(functools.partial(paired_kernel, n, m), out_shape=jax.Shap...  150 us

profile of v3, /device:TPU:16, one launch (start us, length us, event | category | flops | bytes accessed | tf_op | source)
XLA Modules:
  0.0 152.3 jit_solution(17688047167589457310)
XLA Ops:
  0.0 150.0 %shard_map.127 = bf16[256,2048]{1,0:T(8,128)(2,1)} custom-call(bf16[256,2048]{1,0:T(8,128)(2,1)} %skip_ref.1, bf16[1024,256]{1,0:T(8,128)(2,1)} %query_ref.1, bf16[1024,256]{1,0:T(8,128)(2,1)} %forget_ref.1, bf16[1024,256]{1,0:T(8,128)(2,1)} %value_ref.1, bf16[1024,256]{1,0:T(8,128)(2,1)} %emission_ref.1, f32[1,256]{1,0:T(1,128)} %bitcast.4, ...), custom_call_target="tpu_custom_call" | custom-call | tf_op jit(solution)/shard_map/pallas_call | solution.py:1012
  150.0 2.3 %copy.15 = bf16[256,2048]{1,0:T(8,128)(2,1)} copy(bf16[256,2048]{1,0:T(8,128)(2,1)} %shard_map.127) | data formatting | bytes 2097152

commit v4 on v3

--- a/solution.py
+++ b/solution.py
@@ -871,30 +871,48 @@
     for piece in range(pieces):
         normed_arrives(10 + piece, 1, x, 1 - core, piece)
     tiles(1, gate, x)
-    await_weights((1, 0), (1, 4), (1, 6), (1, 5))
-    tiles(0, up)
-    for piece in range(pieces):
-        normed_arrives(6 + piece, 1, 1 - x, core, piece)
-        start(normed_copy(14 + piece, buddy, 1, 1 - x, core, piece))
-    tiles(1, up, x)
+    def collect():
+        for piece in range(pieces):
+            normed_arrives(6 + piece, 1, 1 - x, core, piece)
+            normed_copy(14 + piece, buddy, 1, 1 - x, core, piece).start()
+
+    def collected():
+        for piece in range(pieces):
+            normed_arrives(14 + piece, 1, 1 - x, 1 - core, piece)
+
+    @pl.when(z == 3)
+    def _():
+        collect()
+        collected()
+        tiles(1, gate, 1 - x)
+        await_weights((1, 0), (1, 4), (1, 6), (1, 5))
+        tiles(0, up)
+        tiles(1, up)
 
     @pl.when(z < 3)
     def _():
-        relay(2, 1)
-        forward(2)
-
-    for piece in range(pieces):
-        normed_arrives(14 + piece, 1, 1 - x, 1 - core, piece)
-    tiles(1, gate, 1 - x)
-    tiles(1, up, 1 - x)
-    pl.when(z == 3)(lambda: relay(2, 1))
+        await_weights((1, 0), (1, 4), (1, 6), (1, 5))
+        tiles(0, up)
+        collect()
+        tiles(1, up, x)
+
+        @pl.when(z > 0)
+        def _():
+            relay(2, 1)
+            weight(2, 7, True).start()
+            relay(2, 3)
+
+        collected()
+        tiles(1, gate, 1 - x)
+        tiles(1, up, 1 - x)
 
     base = z // 2
 
     def owner_of(turn):
-        group, even = turn // 2, lax.rem(turn, 2)
-        pair = base + (group // 2) * (1 - 2 * base)
-        return (pair * 2 + even) * 2 + y + lax.rem(group, 2) * (1 - 2 * y)
+        far, second = turn // 4, lax.rem(turn, 4) // 2
+        pair = base + far * (1 - 2 * base)
+        plane = 1 + pair + (1 - lax.rem(far + second, 2)) * (2 * pair - 1)
+        return plane * 2 + y + lax.rem(turn, 2) * (1 - 2 * y)
 
     mine = pl.multiple_of(core * 4 * rows, 4 * rows)
     theirs = pl.multiple_of((1 - core) * 4 * rows, 4 * rows)
@@ -928,32 +946,6 @@
 
     @pl.loop(0, n + lag_plane)
     def _(step):
-        @pl.when(step == 2)
-        def _():
-            await_weights((2, 0), (2, 4))
-            relay(2, 3)
-
-        @pl.when(step == 4)
-        def _():
-            relay(2, 2)
-
-        @pl.when(step == 6)
-        def _():
-            await_weights((2, 5), (2, 6))
-
-        @pl.when(step < n)
-        def _():
-            unit = contraction_half.at[owner_of(step)]
-
-            @pl.loop(0, 4)
-            def _(turn):
-                here = pl.ds(pl.multiple_of(turn * 2 * rows, 2 * rows), 2 * rows)
-                part[step, here, :] = jnp.dot(
-                    hidden[here, :], unit[...], preferred_element_type=F32
-                ).astype(BF16)
-
-            buddy_copy(step).start()
-
         @pl.when((step >= 1) & (step < n + 1))
         def _():
             turn = step - 1
@@ -963,6 +955,36 @@
             cross_out[turn, 1] = share(turn, 1, 1 - x).astype(BF16)
             cross_copy(turn).start()
 
+        def ready(at, outer_needs, inner_needs):
+            def action(big):
+                for kind in inner_needs if big else outer_needs:
+                    if kind in (1, 2, 3):
+                        weight_arrival(2, kind, big).wait_recv()
+                        weight(2, kind + 3, big).start()
+                    else:
+                        weight_arrival(2, kind, big).wait_recv()
+
+            pl.when(step == at)(lambda: by_kind(action))
+
+        ready(1, (0, 1), (4,))
+        ready(2, (2,), ())
+        ready(3, (4, 3), (0, 2))
+        ready(5, (5,), (6,))
+        ready(7, (6,), (5,))
+
+        @pl.when(step < n)
+        def _():
+            unit = contraction_half.at[owner_of(step)]
+
+            @pl.loop(0, 4)
+            def _(turn):
+                here = pl.ds(pl.multiple_of(turn * 2 * rows, 2 * rows), 2 * rows)
+                part[step, here, :] = jnp.dot(
+                    hidden[here, :], unit[...], preferred_element_type=F32
+                ).astype(BF16)
+
+            buddy_copy(step).start()
+
         @pl.when((step >= lag_cross) & (step < n + lag_cross))
         def _():
             turn = step - lag_cross
@@ -989,6 +1011,8 @@
 
     for copy in sends:
         copy.wait_send()
+    for piece in range(pieces):
+        normed_copy(14 + piece, buddy, 1, 1 - x, core, piece).wait_send()
 
     def await_weight_sends(big):
         for tensor in range(3):

time: 152 us -> 147 us (0.967)
  Pallas kernels: 150 us -> 144 us
    pallas_call x1, Pallas kernels: 150 us -> 144 us  [on_device_paired(): pl.pallas_call(functools.partial(paired_kernel, n, m), out_shape=jax.Shap...]
where the time goes in v4:
time: 147 us
  Pallas kernels  144 us (98%)
  local copies, waits for them, and re-layouts  2.3 us (2%)
    pallas_call x1, Pallas kernels, on_device_paired(): pl.pallas_call(functools.partial(paired_kernel, n, m), out_shape=jax.Shap...  144 us

profile of v4, /device:TPU:16, one launch (start us, length us, event | category | flops | bytes accessed | tf_op | source)
XLA Modules:
  0.0 146.8 jit_solution(10116354376826491224)
XLA Ops:
  0.0 144.5 %shard_map.127 = bf16[256,2048]{1,0:T(8,128)(2,1)} custom-call(bf16[256,2048]{1,0:T(8,128)(2,1)} %skip_ref.1, bf16[1024,256]{1,0:T(8,128)(2,1)} %query_ref.1, bf16[1024,256]{1,0:T(8,128)(2,1)} %forget_ref.1, bf16[1024,256]{1,0:T(8,128)(2,1)} %value_ref.1, bf16[1024,256]{1,0:T(8,128)(2,1)} %emission_ref.1, f32[1,256]{1,0:T(1,128)} %bitcast.4, ...), custom_call_target="tpu_custom_call" | custom-call | tf_op jit(solution)/shard_map/pallas_call | solution.py:1036
  144.5 2.3 %copy.15 = bf16[256,2048]{1,0:T(8,128)(2,1)} copy(bf16[256,2048]{1,0:T(8,128)(2,1)} %shard_map.127) | data formatting | bytes 2097152

commit v5 on v4

--- a/solution.py
+++ b/solution.py
@@ -451,12 +451,12 @@
     n,
     m,
     skip_ref,
-    query_ref,
-    forget_ref,
-    value_ref,
-    emission_ref,
+    query_in,
+    forget_in,
+    value_in,
+    emission_in,
     slack_ref,
-    surge_ref,
+    surge_in,
     gain_ref,
     projection_ref,
     row_gain_ref,
@@ -503,6 +503,16 @@
     cross_recv,
     plane_send,
     plane_recv,
+    first_send,
+    first_recv,
+    result,
+    result_sem,
+    query_ref,
+    forget_ref,
+    value_ref,
+    emission_ref,
+    surge_ref,
+    input_sem,
 ):
     sp, tp = lax.axis_index("sp"), lax.axis_index("tp")
     tokens, width = query_ref.shape
@@ -519,6 +529,18 @@
     across = (sp, (1 - x) * 2 + core)
     buddy = (sp, x * 2 + 1 - core)
     paired = (planes[1] * 2 + y, tp)
+
+    first_rows = tokens // 4
+    inputs = [(query_in, query_ref), (forget_in, forget_ref), (surge_in, surge_ref), (value_in, value_ref)]
+    opening, rest = [], []
+    for index, (source, place) in enumerate(inputs):
+        span = pl.ds(0, first_rows)
+        opening.append(pltpu.make_async_copy(source.at[span], place.at[span], input_sem.at[index]))
+        span = pl.ds(first_rows, tokens - first_rows)
+        rest.append(pltpu.make_async_copy(source.at[span], place.at[span], input_sem.at[4 + index]))
+    rest.append(pltpu.make_async_copy(emission_in, emission_ref, input_sem.at[8]))
+    for copy in opening + rest:
+        copy.start()
 
     barrier = pltpu.get_barrier_semaphore()
     for d in range(1, n):
@@ -656,6 +678,8 @@
 
     blocks = tokens // BLOCK
     early = blocks // 4
+    for copy in opening:
+        copy.wait()
     pl.loop(0, early)(recur)
     pl.semaphore_wait(barrier, n - 1 + m - 1)
     send_weights((0, 0))
@@ -672,6 +696,8 @@
         send_weights((1, 1), (1, 3))
 
     start(remote(skip_ref, stream.at[1], skip_sem.at[0], skip_sem.at[1], across))
+    for copy in rest:
+        copy.wait()
     pl.loop(early, blocks)(recur)
 
     for head in range(heads):
@@ -871,41 +897,6 @@
     for piece in range(pieces):
         normed_arrives(10 + piece, 1, x, 1 - core, piece)
     tiles(1, gate, x)
-    def collect():
-        for piece in range(pieces):
-            normed_arrives(6 + piece, 1, 1 - x, core, piece)
-            normed_copy(14 + piece, buddy, 1, 1 - x, core, piece).start()
-
-    def collected():
-        for piece in range(pieces):
-            normed_arrives(14 + piece, 1, 1 - x, 1 - core, piece)
-
-    @pl.when(z == 3)
-    def _():
-        collect()
-        collected()
-        tiles(1, gate, 1 - x)
-        await_weights((1, 0), (1, 4), (1, 6), (1, 5))
-        tiles(0, up)
-        tiles(1, up)
-
-    @pl.when(z < 3)
-    def _():
-        await_weights((1, 0), (1, 4), (1, 6), (1, 5))
-        tiles(0, up)
-        collect()
-        tiles(1, up, x)
-
-        @pl.when(z > 0)
-        def _():
-            relay(2, 1)
-            weight(2, 7, True).start()
-            relay(2, 3)
-
-        collected()
-        tiles(1, gate, 1 - x)
-        tiles(1, up, 1 - x)
-
     base = z // 2
 
     def owner_of(turn):
@@ -929,9 +920,9 @@
     def partner(odd):
         return (sp + (paired[0] - sp) * odd, across[1] + (tp - across[1]) * odd)
 
-    def cross_copy(turn):
-        sems = (cross_send.at[turn], cross_recv.at[turn])
-        return remote(cross_out.at[turn], cross_in.at[turn], *sems, partner(lax.rem(turn, 2)))
+    def cross_copy(turn, which):
+        sems = (cross_send.at[turn * 2 + which], cross_recv.at[turn * 2 + which])
+        return remote(cross_out.at[turn, which], cross_in.at[turn, which], *sems, partner(lax.rem(turn, 2)))
 
     def plane_copy(turn):
         sems = (plane_send.at[turn], plane_recv.at[turn])
@@ -942,18 +933,98 @@
         local_part = part[turn, pl.ds(pl.multiple_of(mine + place, rows), rows), :].astype(F32)
         return local_part + from_buddy[turn, pl.ds(pl.multiple_of(place, rows), rows), :].astype(F32)
 
-    lag_cross, lag_plane = 3, 5
-
-    @pl.loop(0, n + lag_plane)
+    def result_copy(turn):
+        lanes = pl.ds(pl.multiple_of(owner_of(turn) * depth, depth), depth)
+        return pltpu.make_async_copy(result.at[turn], out_ref.at[:, lanes], result_sem.at[turn])
+
+    def down(turn, tile):
+        here = pl.ds(pl.multiple_of(tile * 2 * rows, 2 * rows), 2 * rows)
+        unit = contraction_half.at[owner_of(turn)]
+        part[turn, here, :] = jnp.dot(hidden[here, :], unit[...], preferred_element_type=F32).astype(BF16)
+
+    def first_buddy(plane):
+        place = pl.multiple_of((1 - core) * 4 * rows + plane * 2 * rows, 2 * rows)
+        return remote(
+            part.at[0, pl.ds(place, 2 * rows)],
+            from_buddy.at[0, pl.ds(plane * 2 * rows, 2 * rows)],
+            first_send.at[plane],
+            first_recv.at[plane],
+            buddy,
+        )
+
+    def first_cross(plane):
+        sems = (first_send.at[2 + plane], first_recv.at[2 + plane])
+        return remote(cross_out.at[0, plane], cross_in.at[0, plane], *sems, across)
+
+    def open_first(plane):
+        @pl.loop(0, 2)
+        def _(which):
+            down(0, which * 2 + plane)
+
+        first_buddy(plane).start()
+
+    def close_first(plane):
+        first_buddy(plane).wait_recv()
+        cross_out[0, plane] = share(0, plane, 1 - x).astype(BF16)
+        first_cross(plane).start()
+
+    def collect():
+        for piece in range(pieces):
+            normed_arrives(6 + piece, 1, 1 - x, core, piece)
+            normed_copy(14 + piece, buddy, 1, 1 - x, core, piece).start()
+
+    def collected():
+        for piece in range(pieces):
+            normed_arrives(14 + piece, 1, 1 - x, 1 - core, piece)
+
+    @pl.when(z == 3)
+    def _():
+        collect()
+        collected()
+        tiles(1, gate, 1 - x)
+        await_weights((1, 0), (1, 4), (1, 6), (1, 5))
+        tiles(0, up)
+        open_first(0)
+        tiles(1, up, x)
+        close_first(0)
+        tiles(1, up, 1 - x)
+
+    @pl.when(z < 3)
+    def _():
+        await_weights((1, 0), (1, 4), (1, 6), (1, 5))
+        tiles(0, up)
+        collect()
+        tiles(1, up, x)
+
+        @pl.when(z > 0)
+        def _():
+            relay(2, 1)
+            weight(2, 7, True).start()
+            relay(2, 3)
+
+        open_first(0)
+        collected()
+        tiles(1, gate, 1 - x)
+        close_first(0)
+        tiles(1, up, 1 - x)
+
+    lag_cross, lag_plane = 2, 4
+
+    open_first(1)
+
+    @pl.loop(1, n + lag_plane)
     def _(step):
-        @pl.when((step >= 1) & (step < n + 1))
+        pl.when(step == 1)(lambda: close_first(1))
+
+        @pl.when((step >= 2) & (step < n + 1))
         def _():
             turn = step - 1
             buddy_copy(turn).wait_recv()
             odd = lax.rem(turn, 2)
+            cross_out[turn, 1] = share(turn, 1, 1 - x).astype(BF16)
+            cross_copy(turn, 1).start()
             cross_out[turn, 0] = share(turn, odd, 1 - x + (2 * x - 1) * odd).astype(BF16)
-            cross_out[turn, 1] = share(turn, 1, 1 - x).astype(BF16)
-            cross_copy(turn).start()
+            cross_copy(turn, 0).start()
 
         def ready(at, outer_needs, inner_needs):
             def action(big):
@@ -974,21 +1045,18 @@
 
         @pl.when(step < n)
         def _():
-            unit = contraction_half.at[owner_of(step)]
-
             @pl.loop(0, 4)
-            def _(turn):
-                here = pl.ds(pl.multiple_of(turn * 2 * rows, 2 * rows), 2 * rows)
-                part[step, here, :] = jnp.dot(
-                    hidden[here, :], unit[...], preferred_element_type=F32
-                ).astype(BF16)
+            def _(tile):
+                down(step, tile)
 
             buddy_copy(step).start()
 
         @pl.when((step >= lag_cross) & (step < n + lag_cross))
         def _():
             turn = step - lag_cross
-            cross_copy(turn).wait_recv()
+
+            pl.when(turn == 0)(lambda: first_cross(1).wait_recv())
+            pl.when(turn > 0)(lambda: cross_copy(turn, 1).wait_recv())
             odd = lax.rem(turn, 2)
             total = share(turn, 1 - odd, x + (1 - 2 * x) * odd) + cross_in[turn, 1].astype(F32)
             plane_out[turn] = total.astype(BF16)
@@ -997,17 +1065,29 @@
         @pl.when(step >= lag_plane)
         def _():
             turn = step - lag_plane
+            pl.when(turn == 0)(lambda: first_cross(0).wait_recv())
+            pl.when(turn > 0)(lambda: cross_copy(turn, 0).wait_recv())
             plane_copy(turn).wait_recv()
             lanes = pl.ds(pl.multiple_of(owner_of(turn) * depth, depth), depth)
             total = stream[0, :, lanes].astype(F32) + share(turn, 0, x)
             total += cross_in[turn, 0].astype(F32) + plane_in[turn].astype(F32)
-            out_ref[:, lanes] = total.astype(BF16)
+            result[turn] = total.astype(BF16)
+            result_copy(turn).start()
 
     @pl.loop(0, n)
     def _(turn):
-        buddy_copy(turn).wait_send()
-        cross_copy(turn).wait_send()
+        @pl.when(turn > 0)
+        def _():
+            buddy_copy(turn).wait_send()
+            cross_copy(turn, 0).wait_send()
+            cross_copy(turn, 1).wait_send()
+
         plane_copy(turn).wait_send()
+        result_copy(turn).wait()
+
+    for plane in range(2):
+        first_buddy(plane).wait_send()
+        first_cross(plane).wait_send()
 
     for copy in sends:
         copy.wait_send()
@@ -1036,8 +1116,8 @@
     return pl.pallas_call(
         functools.partial(paired_kernel, n, m),
         out_shape=jax.ShapeDtypeStruct((rows, model), BF16),
-        in_specs=[anywhere] + [vmem] * 7 + [anywhere, vmem] + [anywhere] * 3,
-        out_specs=vmem,
+        in_specs=[anywhere] * 5 + [vmem, anywhere, vmem] + [anywhere, vmem] + [anywhere] * 3,
+        out_specs=anywhere,
         scratch_shapes=[
             pltpu.VMEM((model, many), BF16),
             pltpu.VMEM((model, many), BF16),
@@ -1074,10 +1154,20 @@
             dma((18,)),
             dma((n,)),
             dma((n,)),
+            dma((2 * n,)),
+            dma((2 * n,)),
             dma((n,)),
             dma((n,)),
+            dma((4,)),
+            dma((4,)),
+            pltpu.VMEM((n, rows, depth), BF16),
             dma((n,)),
-            dma((n,)),
+            pltpu.VMEM((tokens, width), BF16),
+            pltpu.VMEM((tokens, width), BF16),
+            pltpu.VMEM((tokens, width), BF16),
+            pltpu.VMEM((tokens, width), BF16),
+            pltpu.VMEM((tokens, width), F32),
+            dma((9,)),
         ],
         compiler_params=pltpu.CompilerParams(
             collective_id=0, has_side_effects=True, vmem_limit_bytes=64_000_000

time: 147 us -> 145 us (0.986)
  Pallas kernels: 144 us -> 142 us
    pallas_call x1, Pallas kernels: 144 us -> 142 us  [on_device_paired(): pl.pallas_call(functools.partial(paired_kernel, n, m), out_shape=jax.Shap...]
where the time goes in v5:
time: 145 us; the launch traced here: 144 us
  Pallas kernels  142 us (98%)
  local copies, waits for them, and re-layouts  2.3 us (2%)
    pallas_call x1, Pallas kernels, on_device_paired(): pl.pallas_call(functools.partial(paired_kernel, n, m), out_shape=jax.Shap...  142 us

profile of v5, /device:TPU:16, one launch (start us, length us, event | category | flops | bytes accessed | tf_op | source)
XLA Modules:
  0.0 144.1 jit_solution(190323733443648435)
XLA Ops:
  0.0 141.8 %shard_map.127 = bf16[256,2048]{1,0:T(8,128)(2,1)} custom-call(bf16[256,2048]{1,0:T(8,128)(2,1)} %skip_ref.1, bf16[1024,256]{1,0:T(8,128)(2,1)} %query_in.1, bf16[1024,256]{1,0:T(8,128)(2,1)} %forget_in.1, bf16[1024,256]{1,0:T(8,128)(2,1)} %value_in.1, bf16[1024,256]{1,0:T(8,128)(2,1)} %emission_in.1, f32[1,256]{1,0:T(1,128)} %bitcast.4, ...), custom_call_target="tpu_custom_call" | custom-call | tf_op jit(solution)/shard_map/pallas_call | solution.py:1116
  141.8 2.3 %copy.15 = bf16[256,2048]{1,0:T(8,128)(2,1)} copy(bf16[256,2048]{1,0:T(8,128)(2,1)} %shard_map.127) | data formatting | bytes 2097152

commit v6 on v5

--- a/solution.py
+++ b/solution.py
@@ -892,11 +892,11 @@
     pass_on(3)
     pl.when(z == 3)(lambda: relay(1, 2))
     send_weights((2, 1), (2, 0))
-    pl.when(outer)(lambda: send_weights((2, 3)))
-    send_weights((2, 2))
     for piece in range(pieces):
         normed_arrives(10 + piece, 1, x, 1 - core, piece)
     tiles(1, gate, x)
+    pl.when(outer)(lambda: send_weights((2, 3)))
+    send_weights((2, 2))
     base = z // 2
 
     def owner_of(turn):
@@ -1008,7 +1008,7 @@
         close_first(0)
         tiles(1, up, 1 - x)
 
-    lag_cross, lag_plane = 2, 4
+    lag_cross, lag_plane = 3, 5
 
     open_first(1)
 
@@ -1026,6 +1026,17 @@
             cross_out[turn, 0] = share(turn, odd, 1 - x + (2 * x - 1) * odd).astype(BF16)
             cross_copy(turn, 0).start()
 
+        @pl.when((step >= lag_cross) & (step < n + lag_cross))
+        def _():
+            turn = step - lag_cross
+
+            pl.when(turn == 0)(lambda: first_cross(1).wait_recv())
+            pl.when(turn > 0)(lambda: cross_copy(turn, 1).wait_recv())
+            odd = lax.rem(turn, 2)
+            total = share(turn, 1 - odd, x + (1 - 2 * x) * odd) + cross_in[turn, 1].astype(F32)
+            plane_out[turn] = total.astype(BF16)
+            plane_copy(turn).start()
+
         def ready(at, outer_needs, inner_needs):
             def action(big):
                 for kind in inner_needs if big else outer_needs:
@@ -1050,17 +1061,6 @@
                 down(step, tile)
 
             buddy_copy(step).start()
-
-        @pl.when((step >= lag_cross) & (step < n + lag_cross))
-        def _():
-            turn = step - lag_cross
-
-            pl.when(turn == 0)(lambda: first_cross(1).wait_recv())
-            pl.when(turn > 0)(lambda: cross_copy(turn, 1).wait_recv())
-            odd = lax.rem(turn, 2)
-            total = share(turn, 1 - odd, x + (1 - 2 * x) * odd) + cross_in[turn, 1].astype(F32)
-            plane_out[turn] = total.astype(BF16)
-            plane_copy(turn).start()
 
         @pl.when(step >= lag_plane)
         def _():

time: 145 us -> 145 us (level)
  no operation moved by 1% of the time
where the time goes in v6:
time: 145 us
  Pallas kernels  142 us (98%)
  local copies, waits for them, and re-layouts  2.3 us (2%)
    pallas_call x1, Pallas kernels, on_device_paired(): pl.pallas_call(functools.partial(paired_kernel, n, m), out_shape=jax.Shap...  142 us

profile of v6, /device:TPU:16, one launch (start us, length us, event | category | flops | bytes accessed | tf_op | source)
XLA Modules:
  0.0 144.6 jit_solution(11192642861533137728)
XLA Ops:
  0.0 142.3 %shard_map.127 = bf16[256,2048]{1,0:T(8,128)(2,1)} custom-call(bf16[256,2048]{1,0:T(8,128)(2,1)} %skip_ref.1, bf16[1024,256]{1,0:T(8,128)(2,1)} %query_in.1, bf16[1024,256]{1,0:T(8,128)(2,1)} %forget_in.1, bf16[1024,256]{1,0:T(8,128)(2,1)} %value_in.1, bf16[1024,256]{1,0:T(8,128)(2,1)} %emission_in.1, f32[1,256]{1,0:T(1,128)} %bitcast.4, ...), custom_call_target="tpu_custom_call" | custom-call | tf_op jit(solution)/shard_map/pallas_call | solution.py:1116
  142.3 2.3 %copy.15 = bf16[256,2048]{1,0:T(8,128)(2,1)} copy(bf16[256,2048]{1,0:T(8,128)(2,1)} %shard_map.127) | data formatting | bytes 2097152
